TPU v7x, 32 devices: a whole 2x2x4 slice. The times are simulated.
32 devices in a mesh: sp: 16 (over z, x, core), tp: 2 (over y).
Axes of the slice: x: 2, y: 2, z: 4, core: 2. Of those that a mesh axis runs over, the one named last changes fastest.
Arguments:
- linear_part: bfloat16 [32768, 2048], P('sp', 'tp'), may hold values from -6 to 6
- gate_part: bfloat16 [32768, 2048], P('sp', 'tp'), may hold values from -8 to 8
- kernel_taps: bfloat16 [31, 2048], P(None, 'tp'), may hold values from -10 to 10
- channel_gain: float32 [2048], replicated, may hold values from 0.1 to 1.9
- output_weight: bfloat16 [2048, 2048], P('tp'), may hold values from -0.125 to 0.125
- residual: bfloat16 [32768, 2048], P(('sp', 'tp')), may hold values from -6 to 6
- mix_gain: float32 [2048], replicated, may hold values from 0.1 to 1.9
- documents: int32 [32768], P('sp'), may hold values from 0 to 3, never falling along the last dimension, each value on 1 to 16384 neighbouring positions
- expert_ids: int32 [32768, 2], P(('sp', 'tp')), may hold values from 0 to 15, all different within a row; in each aligned block of 1024 rows (0 to 1023, 1024 to 2047, ...) at most 512 rows name the same one
- route_weights: float32 [32768, 2], P(('sp', 'tp')), may hold values from 0.25 to 2.5
- expert_gate: bfloat16 [16, 2048, 512], P('sp'), may hold values from -0.125 to 0.125
- expert_up: bfloat16 [16, 2048, 512], P('sp'), may hold values from -0.125 to 0.125
- expert_down: bfloat16 [16, 512, 2048], P('sp'), may hold values from -0.25 to 0.25
- shared_gate: bfloat16 [2048, 256], replicated, may hold values from -0.125 to 0.125
- shared_up: bfloat16 [2048, 256], replicated, may hold values from -0.125 to 0.125
- shared_down: bfloat16 [256, 2048], replicated, may hold values from -0.375 to 0.375
- final_gain: float32 [2048], replicated, may hold values from 0.1 to 1.9
Outputs:
- layer_out: bfloat16 [32768, 2048], P(('sp', 'tp'))
Inputs may be any that keep to these rules, and one draw needn't show every extreme that they name: `expert_ids`: each row names 2 different experts; among the rows of one device (aligned blocks of 1024 rows) no expert is named by more than 512 rows, and exactly 512 in some block. `documents`: never falling along the sequence; each document 1 to 16384 positions.
All inputs are finite; a program needn't handle non-finite values.
Results may differ from a plain program's by a relative error of at most 0.0065.
Values may be sent and summed in bfloat16 or wider, within the bound.
A program may use at most 192 MiB of HBM per device.

v0:
```python
import jax
import jax.numpy as jnp
from jax import lax
from jax.sharding import PartitionSpec as P

EPSILON = 1e-05
RESIDUAL_SCALE = 8.0**0.25


def passed_along(block, axis, distance):
    devices = range(lax.axis_size(axis))
    route = [(i - distance, i) for i in devices if i - distance in devices]
    return lax.ppermute(block, axis, route)


def normalize(values):
    mean = jnp.mean(values, -1, keepdims=True)
    square = jnp.mean(values * values, -1, keepdims=True)
    return (values - mean) * lax.rsqrt(square - mean * mean + EPSILON)


def gathering_is_less(rows, chosen, experts_all, shape):
    weights = experts_all * 3 * shape[1] * shape[2]
    positions = 2 * experts_all * min(rows, 4 * rows * chosen // experts_all) * shape[1]
    return weights <= 2 * positions


def routed_by_weights(normed, expert_ids, route_weights, gates, ups, downs_first, downs_second):
    experts_all, half = downs_first.shape[:2]
    firsts, seconds = [], []
    for expert in range(experts_all):
        weight = jnp.sum(jnp.where(expert_ids == expert, route_weights, 0.0), 1, keepdims=True)
        hidden = jax.nn.silu(
            jnp.dot(normed, gates[expert], preferred_element_type=jnp.float32)
        ) * jnp.dot(normed, ups[expert], preferred_element_type=jnp.float32)
        weighted = (weight * hidden).astype(jnp.bfloat16)
        firsts.append(weighted[:, :half])
        seconds.append(weighted[:, half:])
    width = normed.shape[1]
    return jnp.dot(
        jnp.concatenate(firsts, 1),
        downs_first.reshape(experts_all * half, width),
        preferred_element_type=jnp.float32,
    ) + jnp.dot(
        jnp.concatenate(seconds, 1),
        downs_second.reshape(experts_all * half, width),
        preferred_element_type=jnp.float32,
    )


def routed_by_positions(normed, expert_ids, route_weights, expert_gate, expert_up, expert_down):
    rows = normed.shape[0]
    width_full = normed.shape[1]
    chosen = expert_ids.shape[1]
    experts_all = lax.axis_size("sp") * expert_gate.shape[0]
    capacity = min(rows, 4 * rows * chosen // experts_all)
    flat_ids = expert_ids.reshape(-1)
    onehot = (flat_ids[:, None] == jnp.arange(experts_all, dtype=jnp.int32)[None, :]).astype(
        jnp.int32
    )
    earlier = jnp.cumsum(onehot, 0) - onehot
    ranks = jnp.sum(earlier * onehot, 1)
    slots = flat_ids * capacity + ranks
    places = jnp.arange(experts_all * capacity, dtype=jnp.int32)[:, None] == slots[None, :]
    chooser = jnp.any(places.reshape(experts_all * capacity, rows, chosen), 2).astype(jnp.bfloat16)
    outgoing = jnp.dot(chooser, normed, preferred_element_type=jnp.float32).astype(jnp.bfloat16)
    outgoing = outgoing.reshape(experts_all, capacity, width_full)
    arrived = lax.all_to_all(outgoing, "sp", split_axis=0, concat_axis=0, tiled=True)
    sources, items, width = arrived.shape
    flat = arrived.reshape(sources * items, width)
    hidden = (
        jax.nn.silu(jnp.dot(flat, expert_gate[0], preferred_element_type=jnp.float32))
        * jnp.dot(flat, expert_up[0], preferred_element_type=jnp.float32)
    ).astype(jnp.bfloat16)
    answer = jnp.dot(hidden, expert_down[0], preferred_element_type=jnp.float32).astype(
        jnp.bfloat16
    )
    answered = answer.reshape(sources, items, width)
    returned = lax.all_to_all(answered, "sp", split_axis=0, concat_axis=0, tiled=True).reshape(
        experts_all * capacity, width_full
    )
    picked = jnp.take(returned, slots, axis=0).astype(jnp.float32).reshape(rows, chosen, width_full)
    return jnp.sum(picked * route_weights[:, :, None], 1)


def shards(
    linear_part,
    gate_part,
    kernel_taps,
    channel_gain,
    output_weight,
    residual,
    mix_gain,
    documents,
    expert_ids,
    route_weights,
    expert_gate,
    expert_up,
    expert_down,
    shared_gate,
    shared_up,
    shared_down,
    final_gain,
):
    experts_all = lax.axis_size("sp") * expert_gate.shape[0]
    gathers = gathering_is_less(residual.shape[0], expert_ids.shape[1], experts_all, expert_gate.shape)
    weight_all = lax.all_gather(output_weight, "tp", axis=0, tiled=True)
    if gathers:
        half = expert_down.shape[1] // 2
        weight_all, expert_gate, expert_up, first, second = lax.optimization_barrier(
            (weight_all, expert_gate, expert_up, expert_down[:, :half], expert_down[:, half:])
        )
        gates, ups, downs_first, downs_second = [
            lax.all_gather(part, "sp", axis=0, tiled=True)
            for part in (expert_gate, expert_up, first, second)
        ]
    reach = kernel_taps.shape[0] - 1
    length = linear_part.shape[0]
    gated = (
        linear_part.astype(jnp.float32) * jax.nn.sigmoid(gate_part.astype(jnp.float32))
    ).astype(jnp.bfloat16)
    before, before_docs = passed_along(
        (gated[length - reach :], documents[length - reach :]), "sp", 1
    )
    extended = jnp.concatenate([before, gated], 0)
    extended_docs = jnp.concatenate([before_docs, documents], 0)
    taps = kernel_taps.astype(jnp.float32)
    total = jnp.zeros(gated.shape, jnp.float32)
    for offset in range(reach + 1):
        window = lax.slice_in_dim(extended, reach - offset, reach - offset + length, axis=0).astype(
            jnp.float32
        )
        same = (
            lax.slice_in_dim(extended_docs, reach - offset, reach - offset + length, axis=0)
            == documents
        )
        total = total + jnp.where(same[:, None], window * taps[offset], 0.0)
    convolved = total.astype(jnp.bfloat16)
    position_rows = lax.all_to_all(convolved, "tp", split_axis=0, concat_axis=1, tiled=True)
    activated = jax.nn.silu(normalize(position_rows.astype(jnp.float32)) * channel_gain).astype(
        jnp.bfloat16
    )
    projected = jnp.dot(
        activated,
        weight_all,
        preferred_element_type=jnp.float32,
    )
    normed = (
        normalize(RESIDUAL_SCALE * residual.astype(jnp.float32) + projected) * mix_gain
    ).astype(jnp.bfloat16)
    if gathers:
        routed = routed_by_weights(
            normed, expert_ids, route_weights, gates, ups, downs_first, downs_second
        )
    else:
        routed = routed_by_positions(
            normed, expert_ids, route_weights, expert_gate, expert_up, expert_down
        )
    common = (
        jax.nn.silu(jnp.dot(normed, shared_gate, preferred_element_type=jnp.float32))
        * jnp.dot(normed, shared_up, preferred_element_type=jnp.float32)
    ).astype(jnp.bfloat16)
    shared_out = jnp.dot(common, shared_down, preferred_element_type=jnp.float32)
    return (
        normalize(RESIDUAL_SCALE * normed.astype(jnp.float32) + routed + shared_out) * final_gain
    ).astype(jnp.bfloat16)


def solution(mesh):
    return jax.shard_map(
        shards,
        mesh=mesh,
        in_specs=(
            P("sp", "tp"),
            P("sp", "tp"),
            P(None, "tp"),
            P(),
            P("tp", None),
            P(("sp", "tp"), None),
            P(),
            P("sp"),
            P(("sp", "tp"), None),
            P(("sp", "tp"), None),
            P("sp", None, None),
            P("sp", None, None),
            P("sp", None, None),
            P(),
            P(),
            P(),
            P(),
        ),
        out_specs=P(("sp", "tp"), None),
        check_vma=False,
    )
```

profile of v0, /device:TPU:0, one launch (start us, length us, event | category | flops | bytes accessed | tf_op | source)
XLA Modules:
  0.0 747.1 jit_solution(16791511272193930489)
XLA Ops:
  8.2 1.5 fusion.150
  9.7 105.9 %all-gather.6.cloned.1.call-done = bf16[2048,2048]{1,0:T(8,128)(2,1)} async-done(((bf16[1024,2048]{1,0:T(8,128)(2,1)}), bf16[2048,2048]{1,0:T(8,128)(2,1)}) %all-gather.6.cloned.1.call-update) | async-done | bytes 8388624 | tf_op jit(solution)/shard_map/all_gather | solution.py:107
  117.0 1.7 collective-permute-start
  118.7 5.0 multiply_convert_fusion.3
  123.7 2.0 copy-done.4
  125.8 3.8 collective-permute-start.1
  130.5 100.2 %add_convert_fusion = bf16[2048,1024]{1,0:T(8,128)(2,1)} fusion(bf16[2048,1024]{1,0:T(8,128)(2,1)} %copy-done.4, bf16[30,1024]{1,0:T(8,128)(2,1)S(1)} %collective-permute-done.1, f32[1024]{0:T(1024)S(1)} %bitcast.247, f32[1024]{0:T(1024)S(1)} %bitcast.246, f32[1024]{0:T(1024)S(1)} %bitcast.245, f32[1024]{0:T(1024)S(1)} %bitcast.244, f32[1024]{0:T(1024)S(1)} %bitcast.243, ...), kind=kLoop, calls=%fused_computation.42 | loop fusion | flops 446693376 | bytes 8638464 | tf_op jit(solution)/shard_map/convert_element_type | solution.py:138
  230.7 5.7 all-to-all-start
  237.7 46.5 %all-to-all-done = bf16[2,1024,1024]{2,1,0:T(8,128)(2,1)} async-done(((bf16[2,1024,1024]{2,1,0:T(8,128)(2,1)}), bf16[2,1024,1024]{2,1,0:T(8,128)(2,1)}, u32[]{:S(2)}, u32[]{:S(2)}) %all-to-all-start) | async-done | bytes 4194336 | tf_op jit(solution)/shard_map/all_to_all | solution.py:139
  284.2 6.5 convert_bitcast_fusion
  290.7 9.1 %copy.19 = f32[1024,2,1024]{0,2,1:T(8,128)} copy(f32[1024,2,1024]{2,0,1:T(8,128)} %convert_bitcast_fusion) | data formatting | bytes 16777216 | tf_op jit(solution)/shard_map/convert_element_type | solution.py:140
  299.9 3.6 convert_reduce_fusion
  303.5 5.0 multiply_convert_fusion.2
  308.5 1.2 slice-done.1
  309.7 10.5 %fusion.149 = (f32[1024]{0:T(1024)S(1)}, f32[1024]{0:T(1024)S(1)}, f32[1024,2048]{1,0:T(8,128)S(1)}) fusion(bf16[1024,2048]{0,1:T(8,128)(2,1)S(1)} %multiply_convert_fusion.2, bf16[2048,2048]{1,0:T(8,128)(2,1)S(1)} %bitcast.250, bf16[1024,2048]{1,0:T(8,128)(2,1)S(1)} %copy-done.22), kind=kOutput, calls=%fused_computation.358 | convolution fusion | flops 8602515456 | bytes 25174016 | tf_op jit(solution)/shard_map/dot_general | solution.py:143
  320.3 1.6 multiply_convert_fusion.1
  321.9 2.0 copy-done.2
  323.9 1.3 fusion.154
  325.2 10.0 %fusion.65 = f32[1024,2048]{1,0:T(8,128)} fusion(bf16[256,2048]{1,0:T(8,128)(2,1)S(1)} %copy-done, bf16[1024,2048]{1,0:T(8,128)(2,1)} %copy-done.2, bf16[2048,256]{1,0:T(8,128)(2,1)S(1)} %copy-done.6, f32[1024,256]{1,0:T(8,128)S(1)} %fusion.154), kind=kOutput, calls=%fused_computation.161 | convolution fusion | flops 2149056512 | bytes 15728640 | tf_op jit(solution)/shard_map/dot_general | solution.py:163
  335.2 5.5 fusion.63
  340.7 115.0 %all-gather.10.cloned.1.call-done = bf16[16,2048,512]{2,1,0:T(8,128)(2,1)} async-done(((bf16[1,2048,512]{2,1,0:T(8,128)(2,1)}), bf16[16,2048,512]{2,1,0:T(8,128)(2,1)}) %all-gather.10.cloned.1.call-update) | async-done | bytes 33554448 | tf_op jit(solution)/shard_map/all_gather | solution.py:114
  455.6 5.6 multiply_convert_fusion.19
  462.3 4.0 fusion.61
  466.3 4.7 multiply_convert_fusion.18
  471.0 1.1 slice_dynamic-update-slice_fusion.14
  472.1 4.0 fusion.59
  476.1 4.3 multiply_convert_fusion.17
  481.4 4.0 fusion.57
  485.4 4.3 multiply_convert_fusion.16
  490.8 4.4 fusion.55
  495.2 4.3 multiply_convert_fusion.15
  499.5 1.1 slice_dynamic-update-slice_fusion.11
  500.6 4.0 fusion.53
  504.6 4.3 multiply_convert_fusion.14
  509.9 4.5 fusion.51
  514.3 4.5 multiply_convert_fusion.13
  518.8 1.1 slice_dynamic-update-slice_fusion.9
  519.9 4.0 fusion.49
  523.9 4.3 multiply_convert_fusion.12
  529.3 4.0 fusion.47
  533.3 4.3 multiply_convert_fusion.11
  537.6 1.1 slice_dynamic-update-slice_fusion.7
  538.7 4.2 fusion.45
  542.9 4.3 multiply_convert_fusion.10
  547.2 1.1 slice_dynamic-update-slice_fusion.6
  548.3 4.0 fusion.43
  552.3 4.3 multiply_convert_fusion.9
  556.6 1.1 slice_dynamic-update-slice_fusion.5
  557.7 4.0 fusion.41
  561.7 4.7 multiply_convert_fusion.8
  567.5 4.0 fusion.39
  571.5 4.3 multiply_convert_fusion.7
  576.8 4.0 fusion.37
  580.9 4.3 multiply_convert_fusion.6
  586.2 4.2 fusion.35
  590.4 4.5 multiply_convert_fusion.5
  594.9 1.1 slice_dynamic-update-slice_fusion.1
  596.0 4.0 fusion.33
  600.0 4.3 multiply_convert_fusion.4
  604.3 1.1 slice_dynamic-update-slice_fusion
  605.4 24.2 %fusion.153 = f32[1024,2048]{1,0:T(8,128)} fusion(bf16[1024,4096]{0,1:T(8,128)(2,1)} %get-tuple-element.40, bf16[4096,2048]{1,0:T(8,128)(2,1)} %bitcast.248), kind=kOutput, calls=%fused_computation.362 | convolution fusion | flops 17179869184 | bytes 33554432 | tf_op jit(solution)/shard_map/dot_general | solution.py:40
  629.6 81.1 %all-gather.14.cloned.1.call-done = bf16[16,256,2048]{2,1,0:T(8,128)(2,1)} async-done(((bf16[1,256,2048]{2,1,0:T(8,128)(2,1)}), bf16[16,256,2048]{2,1,0:T(8,128)(2,1)}) %all-gather.14.cloned.1.call-update) | async-done | bytes 16777232 | tf_op jit(solution)/shard_map/all_gather | solution.py:114
  710.8 26.8 %fusion.148 = (f32[1024]{0:T(1024)S(1)}, f32[1024]{0:T(1024)S(1)}, f32[1024,2048]{1,0:T(8,128)S(1)}) fusion(f32[1024,2048]{1,0:T(8,128)} %fusion.65, f32[1024,2048]{1,0:T(8,128)} %fusion.153, bf16[1024,4096]{0,1:T(8,128)(2,1)} %get-tuple-element.39, bf16[4096,2048]{1,0:T(8,128)(2,1)} %bitcast.215, bf16[1024,2048]{1,0:T(8,128)(2,1)} %copy-done.2), kind=kOutput, calls=%fused_computation.357 | convolution fusion | flops 17196646400 | bytes 54534144 | tf_op jit(solution)/shard_map/dot_general | solution.py:44
  737.6 2.7 multiply_convert_fusion
  (84 shorter events, 13.5 us)
Async XLA Ops:
  6.5 318.6 %copy-start = (bf16[256,2048]{1,0:T(8,128)(2,1)S(1)}, bf16[256,2048]{1,0:T(8,128)(2,1)}, u32[]{:S(2)}) copy-start(bf16[256,2048]{1,0:T(8,128)(2,1)} %param.32) | copy-start | bytes 3145732
  6.5 1.7 copy-start.5
  6.5 109.1 %all-gather.6.cloned.1.call-start = ((), (), s32[]{:S(2)}) async-start(), calls=%async_computation.1 | async-start | bytes 12582912 | tf_op jit(solution)/shard_map/all_gather | solution.py:107
  7.3 109.7 %copy-start.8 = (s32[2048]{0:T(1024)S(1)}, s32[2048]{0:T(1024)}, u32[]{:S(2)}) copy-start(s32[2048]{0:T(1024)} %param.24) | copy-start | bytes 24580
  7.3 327.9 %all-gather.8.cloned.1.call-start = ((), (), s32[]{:S(2)}) async-start(), calls=%async_computation.2 | async-start | bytes 35651584 | tf_op jit(solution)/shard_map/all_gather | solution.py:114
  115.6 340.0 %all-gather.10.cloned.1.call-start = ((), (), s32[]{:S(2)}) async-start(), calls=%async_computation.3 | async-start | bytes 35651584 | tf_op jit(solution)/shard_map/all_gather | solution.py:114
  116.4 489.0 %all-gather.12.cloned.1.call-start = ((), (), s32[]{:S(2)}) async-start(), calls=%async_computation.4 | async-start | bytes 17825792 | tf_op jit(solution)/shard_map/all_gather | solution.py:114
  117.0 12.6 %copy-start.7 = (bf16[31,1024]{1,0:T(8,128)(2,1)S(1)}, bf16[31,1024]{1,0:T(8,128)(2,1)}, u32[]{:S(2)}) copy-start(bf16[31,1024]{1,0:T(8,128)(2,1)} %param.19) | copy-start | bytes 190468
  117.0 12.7 %collective-permute-start = (s32[30]{0:T(128)S(1)}, s32[30]{0:T(128)S(1)}, u32[]{:S(2)}, u32[]{:S(2)}) collective-permute-start(s32[30]{0:T(128)S(1)} %slice.478), channel_id=1, source_target_pairs={{0,2},{2,4},{4,6},{6,8},{8,10},{10,12},{12,14},{14,16},{16,18},{18... | collective-permute-start | bytes 368 | tf_op jit(solution)/shard_map/ppermute | solution.py:13
  123.7 2.0 copy-start.4
  125.8 4.7 collective-permute-start.1
  230.7 6.2 copy-start.12
  230.7 6.2 copy-start.13
  230.7 53.4 %all-to-all-start = ((bf16[2,1024,1024]{2,1,0:T(8,128)(2,1)}), bf16[2,1024,1024]{2,1,0:T(8,128)(2,1)}, u32[]{:S(2)}, u32[]{:S(2)}) async-start(bf16[2,1024,1024]{2,1,0:T(8,128)(2,1)} %bitcast.216), calls=%async_computation | async-start | bytes 8388608 | tf_op jit(solution)/shard_map/all_to_all | solution.py:139
  236.4 474.3 %all-gather.14.cloned.1.call-start = ((), (), s32[]{:S(2)}) async-start(), calls=%async_computation.5 | async-start | bytes 17825792 | tf_op jit(solution)/shard_map/all_gather | solution.py:114
  299.9 3.6 copy-start.9
  299.9 8.7 %slice-start = ((s8[8388608]{0:T(1024)(128)(4,1)}), s8[4194304]{0:T(1024)(128)(4,1)S(1)}, s32[]{:S(2)}) async-start(s8[8388608]{0:T(1024)(128)(4,1)} %bitcast.249), calls=%async_computation.6 | async-start | bytes 8388608
  303.5 6.2 slice-start.1
  303.5 6.2 copy-start.22
  309.7 10.5 %copy-start.10 = (f32[2048]{0:T(1024)S(1)}, f32[2048]{0:T(1024)}, u32[]{:S(2)}) copy-start(f32[2048]{0:T(1024)} %param.23) | copy-start | bytes 24580
  320.3 3.6 copy-start.23
  321.9 2.0 copy-start.2
  323.9 1.3 copy-start.6
  455.6 6.7 copy-start.3
  529.3 4.0 copy-start.21
  538.7 4.3 copy-start.20
  548.3 4.0 copy-start.19
  557.7 4.1 copy-start.18
  567.5 4.0 copy-start.17
  576.8 4.0 copy-start.16
  586.2 4.2 copy-start.15
  596.0 4.0 copy-start.14
  710.8 26.9 %copy-start.11 = (f32[2048]{0:T(1024)S(1)}, f32[2048]{0:T(1024)}, u32[]{:S(2)}) copy-start(f32[2048]{0:T(1024)} %param.33) | copy-start | bytes 24580
  737.6 2.8 copy-start.1
Sparse Core Ops, SparseCore 0:
  8.9 106.6 all-gather.5
  117.2 168.0 all-gather.7
  286.9 168.7 all-gather.9
  457.7 126.3 all-gather.11
  586.1 124.5 all-gather.13
where the time goes:
time: 755 us; the launch traced here: 747 us
  waiting for transfers between devices  351 us (46%)
  matrix products  211 us (28%)
  other arithmetic  126 us (17%)
  local copies, waits for them, and re-layouts  33.7 us (4%)
  between operations  14 us (2%)
  starting transfers between devices  11.8 us (2%)
    all_gather x4, waiting for transfers between devices, shards(): lax.all_gather(part, 'sp', axis=0, tiled=True)  196 us
    all_gather x1, waiting for transfers between devices, shards(): weight_all = lax.all_gather(output_weight, 'tp', axis=0, tiled=True)  106 us
    convert_element_type x1, other arithmetic, shards(): convolved = total.astype(jnp.bfloat16)  100 us
    dot_general x16, matrix products, routed_by_weights(): jnp.dot(normed, ups[expert], preferred_element_type=jnp.float32)  71.2 us
    dot_general x16, matrix products, routed_by_weights(): jnp.dot(normed, gates[expert], preferred_element_type=jnp.float32)  66.9 us
    all_to_all x1, waiting for transfers between devices, shards(): lax.all_to_all(convolved, 'tp', split_axis=0, concat_axis=1, tiled=True)  46.5 us
    dot_general x1, matrix products, routed_by_weights(): jnp.dot(jnp.concatenate(seconds, 1), downs_second.reshape(experts_all * h...  26.8 us
    dot_general x1, matrix products, routed_by_weights(): jnp.dot(jnp.concatenate(firsts, 1), downs_first.reshape(experts_all * hal...  24.2 us
  transfers between devices with their start and end apart: 8, of which 5 were waited for; matrix products, arithmetic and copies ran while one was open for 45% of the time, Pallas kernels for 0%

commit v1 on v0

--- a/solution.py
+++ b/solution.py
@@ -1,6 +1,10 @@
+import functools
+
 import jax
 import jax.numpy as jnp
 from jax import lax
+from jax.experimental import pallas as pl
+from jax.experimental.pallas import tpu as pltpu
 from jax.sharding import PartitionSpec as P
 
 EPSILON = 1e-05
@@ -83,7 +87,7 @@
     return jnp.sum(picked * route_weights[:, :, None], 1)
 
 
-def shards(
+def shards_any(
     linear_part,
     gate_part,
     kernel_taps,
@@ -166,6 +170,437 @@
     ).astype(jnp.bfloat16)
 
 
+HALO = 32
+LANES = 128
+PIECE = 128
+
+
+def column_of(table, lane):
+    lanes = lax.broadcasted_iota(jnp.int32, table.shape, 1)
+    return jnp.sum(jnp.where(lanes == lane, table, 0.0), 1, keepdims=True)
+
+
+def conv_kernel(taps, part_ref, lin_ref, gate_ref, lin_back_ref, gate_back_ref, halo_ref, tap_ref, runs_ref, short_ref, out_ref, held):
+    rows = out_ref.shape[0]
+
+    def gated_of(lin, gate):
+        lin = lin.astype(jnp.float32)
+        gate = gate.astype(jnp.float32)
+        return (lin * jax.nn.sigmoid(gate)).astype(jnp.bfloat16).astype(jnp.float32)
+
+    @pl.when(part_ref[0] == 0)
+    def _():
+        held[0:HALO] = halo_ref[...].astype(jnp.float32)
+
+    @pl.when(part_ref[0] != 0)
+    def _():
+        held[0:HALO] = gated_of(lin_back_ref[...], gate_back_ref[...])
+
+    @pl.loop(0, rows // LANES)
+    def _(i):
+        at = pl.multiple_of(i * LANES, LANES)
+        held[pl.ds(pl.multiple_of(HALO + at, HALO), LANES)] = gated_of(
+            lin_ref[pl.ds(at, LANES)], gate_ref[pl.ds(at, LANES)]
+        )
+
+    step = 64
+
+    @pl.loop(0, rows // step)
+    def _(i):
+        at = pl.multiple_of(i * step, step)
+
+        def summed(masked):
+            total = jnp.zeros((step, LANES), jnp.float32)
+            run = runs_ref[pl.ds(at, step)] if masked else None
+            for offset in range(taps):
+                window = held[pl.ds(at + (HALO - offset), step)]
+                term = window * tap_ref[offset : offset + 1]
+                if masked:
+                    term = jnp.where(run >= offset, term, 0.0)
+                total = total + term
+            out_ref[pl.ds(at, step)] = total.astype(out_ref.dtype)
+
+        short = short_ref[i] != 0
+
+        @pl.when(short)
+        def _():
+            summed(True)
+
+        @pl.when(jnp.logical_not(short))
+        def _():
+            summed(False)
+
+
+def convolve(part, linear_part, gate_part, halo, taps, runs, short):
+    rows = linear_part.shape[0] // 2
+    width = linear_part.shape[1]
+    back = rows // HALO
+    block = lambda of: pl.BlockSpec((rows, LANES), of)
+    return pl.pallas_call(
+        functools.partial(conv_kernel, taps.shape[0]),
+        out_shape=jax.ShapeDtypeStruct((rows, width), jnp.bfloat16),
+        grid_spec=pltpu.PrefetchScalarGridSpec(
+            num_scalar_prefetch=1,
+            grid=(width // LANES,),
+            in_specs=[
+                block(lambda c, part: (part[0], c)),
+                block(lambda c, part: (part[0], c)),
+                pl.BlockSpec((HALO, LANES), lambda c, part: (part[0] * back - part[0], c)),
+                pl.BlockSpec((HALO, LANES), lambda c, part: (part[0] * back - part[0], c)),
+                pl.BlockSpec((HALO, LANES), lambda c, part: (0, c)),
+                pl.BlockSpec((taps.shape[0], LANES), lambda c, part: (0, c)),
+                block(lambda c, part: (0, 0)),
+                pl.BlockSpec(memory_space=pltpu.SMEM),
+            ],
+            out_specs=block(lambda c, part: (0, c)),
+            scratch_shapes=[pltpu.VMEM((HALO + rows, LANES), jnp.float32)],
+        ),
+        cost_estimate=pl.CostEstimate(
+            flops=rows * width * taps.shape[0] * 12, bytes_accessed=rows * width * 6, transcendentals=0
+        ),
+        compiler_params=pltpu.CompilerParams(dimension_semantics=("arbitrary",)),
+        name="convolve",
+    )(part, linear_part, gate_part, linear_part, gate_part, halo, taps, runs, short)
+
+
+def row_norm(values):
+    width = values.shape[1]
+    mean = jnp.sum(values, 1, keepdims=True) * (1.0 / width)
+    square = jnp.sum(values * values, 1, keepdims=True) * (1.0 / width)
+    return (values - mean) * lax.rsqrt(square - mean * mean + EPSILON)
+
+
+def project_kernel(own_ref, came_ref, own_gain_ref, came_gain_ref, w_own_ref, w_came_ref, residual_ref, gain_ref, *refs):
+    out_ref = refs[-1]
+    own = own_ref[...].astype(jnp.float32)
+    came = came_ref[...].astype(jnp.float32)
+    width = own.shape[1] + came.shape[1]
+    mean = (jnp.sum(own, 1, keepdims=True) + jnp.sum(came, 1, keepdims=True)) * (1.0 / width)
+    square = (
+        jnp.sum(own * own, 1, keepdims=True) + jnp.sum(came * came, 1, keepdims=True)
+    ) * (1.0 / width)
+    scale = lax.rsqrt(square - mean * mean + EPSILON)
+    own = jax.nn.silu((own - mean) * scale * own_gain_ref[...]).astype(jnp.bfloat16)
+    came = jax.nn.silu((came - mean) * scale * came_gain_ref[...]).astype(jnp.bfloat16)
+    projected = jnp.dot(own, w_own_ref[...], preferred_element_type=jnp.float32) + jnp.dot(
+        came, w_came_ref[...], preferred_element_type=jnp.float32
+    )
+    mixed = RESIDUAL_SCALE * residual_ref[...].astype(jnp.float32) + projected
+    out_ref[...] = (row_norm(mixed) * gain_ref[...]).astype(out_ref.dtype)
+
+
+def project(first, count, own, came, own_gain, came_gain, w_own, w_came, residual, gain, before):
+    total_rows, width = residual.shape
+    half = own.shape[1]
+    rows = min(count, 256)
+    start = first // rows
+    whole = lambda shape: pl.BlockSpec(shape, lambda r: (0, 0))
+    here = lambda columns: pl.BlockSpec((rows, columns), lambda r: (r + start, 0))
+    in_specs = [
+        here(half),
+        here(half),
+        whole((1, half)),
+        whole((1, half)),
+        whole((half, width)),
+        whole((half, width)),
+        here(width),
+        whole((1, width)),
+    ]
+    operands = [own, came, own_gain, came_gain, w_own, w_came, residual, gain]
+    if before is not None:
+        in_specs.append(pl.BlockSpec(memory_space=pl.ANY))
+        operands.append(before)
+    return pl.pallas_call(
+        project_kernel,
+        out_shape=jax.ShapeDtypeStruct((total_rows, width), jnp.bfloat16),
+        grid=(count // rows,),
+        in_specs=in_specs,
+        out_specs=here(width),
+        input_output_aliases={} if before is None else {8: 0},
+        cost_estimate=pl.CostEstimate(
+            flops=2 * count * width * width, bytes_accessed=4 * half * width + 6 * count * width, transcendentals=0
+        ),
+        compiler_params=pltpu.CompilerParams(dimension_semantics=("arbitrary",)),
+        name="project",
+    )(*operands)
+
+
+def experts_kernel(group, piece, has_start, later, start_at, x_ref, table_ref, w_ref, *refs):
+    start_ref = refs[0] if has_start else None
+    out_ref, total, in_sem, out_sem = refs[has_start + later :]
+    rows, width = x_ref.shape
+    step = pl.program_id(0)
+    last = pl.num_programs(0) - 1
+    tile = min(rows, 512)
+    wide = 2 * piece
+
+    @pl.when(step == 0)
+    def _():
+        if has_start:
+            copy = pltpu.make_async_copy(start_ref.at[pl.ds(start_at, rows)], total, in_sem)
+            copy.start()
+            copy.wait()
+        else:
+            total[...] = jnp.zeros_like(total)
+
+    @pl.loop(0, rows // tile)
+    def _(i):
+        at = pl.ds(pl.multiple_of(i * tile, tile), tile)
+        x = x_ref[at]
+        table = table_ref[at]
+        hidden = []
+        for member in range(group):
+            both = jnp.dot(x, w_ref[member, :width], preferred_element_type=jnp.float32)
+            gate, up = both[:, :piece], both[:, piece:]
+            weight = column_of(table, step * group + member)
+            hidden.append((jax.nn.silu(gate) * up * weight).astype(jnp.bfloat16))
+        hidden = jnp.concatenate(hidden, 1)
+        for block in range(width // wide):
+            low = width + block * piece
+            down = jnp.concatenate([w_ref[member, low : low + piece] for member in range(group)], 0)
+            columns = slice(block * wide, (block + 1) * wide)
+            total[at, columns] += jnp.dot(hidden, down, preferred_element_type=jnp.float32)
+
+    @pl.when(step == last)
+    def _():
+        if out_ref.dtype == jnp.float32:
+            copy = pltpu.make_async_copy(total, out_ref, out_sem)
+            copy.start()
+            copy.wait()
+        else:
+            out_ref[...] = total[...].astype(out_ref.dtype)
+
+
+def experts(at, x, table, weights, start, dtype, after=()):
+    first, count = at
+    width = x.shape[1]
+    experts_all, depth, wide = weights.shape
+    piece = wide // 2
+    group = 4 if experts_all % 4 == 0 else experts_all
+    here = first // count
+    anywhere = pl.BlockSpec(memory_space=pl.ANY)
+    in_specs = [
+        pl.BlockSpec((count, width), lambda e: (here, 0)),
+        pl.BlockSpec((count, LANES), lambda e: (here, 0)),
+        pl.BlockSpec((group, depth, wide), lambda e: (e, 0, 0)),
+    ]
+    operands = [x, table, weights]
+    if start is not None:
+        operands.append(start)
+    operands.extend(after)
+    in_specs.extend([anywhere] * (len(operands) - 3))
+    kept = dtype == jnp.float32
+    return pl.pallas_call(
+        functools.partial(experts_kernel, group, piece, start is not None, len(after), first),
+        out_shape=jax.ShapeDtypeStruct((count, width), dtype),
+        grid=(experts_all // group,),
+        in_specs=in_specs,
+        out_specs=anywhere if kept else pl.BlockSpec((count, width), lambda e: (0, 0)),
+        scratch_shapes=[
+            pltpu.VMEM((count, width), jnp.float32),
+            pltpu.SemaphoreType.DMA,
+            pltpu.SemaphoreType.DMA,
+        ],
+        cost_estimate=pl.CostEstimate(
+            flops=2 * count * experts_all * depth * wide,
+            bytes_accessed=2 * experts_all * depth * wide + 8 * count * width,
+            transcendentals=0,
+        ),
+        compiler_params=pltpu.CompilerParams(
+            dimension_semantics=("arbitrary",), vmem_limit_bytes=56 * 1024 * 1024
+        ),
+        name="experts",
+    )(*operands)
+
+
+def finish_kernel(normed_ref, routed_ref, shared_ref, came_ref, gain_ref, *refs):
+    mixed = RESIDUAL_SCALE * normed_ref[...].astype(jnp.float32) + routed_ref[...]
+    mixed = mixed + shared_ref[...] + came_ref[...].astype(jnp.float32)
+    refs[-1][...] = (row_norm(mixed) * gain_ref[...]).astype(jnp.bfloat16)
+
+
+def finish(first, normed, routed, shared, came, gain, before):
+    rows, width = normed.shape
+    count = came.shape[0]
+    tile = 128
+    start = first // tile
+    here = pl.BlockSpec((tile, width), lambda r: (r + start, 0))
+    in_specs = [here, here, here, pl.BlockSpec((tile, width), lambda r: (r, 0)), pl.BlockSpec((1, width), lambda r: (0, 0))]
+    operands = [normed, routed, shared, came, gain]
+    if before is not None:
+        in_specs.append(pl.BlockSpec(memory_space=pl.ANY))
+        operands.append(before)
+    return pl.pallas_call(
+        finish_kernel,
+        out_shape=jax.ShapeDtypeStruct((rows, width), jnp.bfloat16),
+        grid=(count // tile,),
+        in_specs=in_specs,
+        out_specs=here,
+        input_output_aliases={} if before is None else {5: 0},
+        cost_estimate=pl.CostEstimate(
+            flops=10 * count * width, bytes_accessed=14 * count * width, transcendentals=0
+        ),
+        compiler_params=pltpu.CompilerParams(dimension_semantics=("arbitrary",)),
+        name="finish",
+    )(*operands)
+
+
+def packed(gate, up, down, low):
+    width = gate.shape[0]
+    blocks = width // (2 * PIECE)
+    both = jnp.concatenate(
+        [lax.dynamic_slice_in_dim(gate, low, PIECE, 1), lax.dynamic_slice_in_dim(up, low, PIECE, 1)], 1
+    )
+    below = lax.dynamic_slice_in_dim(down, low, PIECE, 0)
+    below = below.reshape(PIECE, blocks, 2 * PIECE).transpose(1, 0, 2).reshape(blocks * PIECE, 2 * PIECE)
+    return jnp.concatenate([both, below], 0)[None]
+
+
+def swapped(block, axis):
+    return lax.ppermute(block, axis, [(i, i ^ 1) for i in range(lax.axis_size(axis))])
+
+
+def weight_table(names, weights):
+    lanes = jnp.arange(LANES, dtype=jnp.float32)[None, :]
+    return sum(
+        jnp.where(names[k][:, None] == lanes, weights[k][:, None], 0.0) for k in range(names.shape[0])
+    )
+
+
+def shards_split(
+    linear_part,
+    gate_part,
+    kernel_taps,
+    channel_gain,
+    output_weight,
+    residual,
+    mix_gain,
+    documents,
+    expert_ids,
+    route_weights,
+    expert_gate,
+    expert_up,
+    expert_down,
+    shared_gate,
+    shared_up,
+    shared_down,
+    final_gain,
+):
+    mine = lax.axis_index("tp")
+    other = 1 - mine
+    reach = kernel_taps.shape[0] - 1
+    length = linear_part.shape[0]
+    rows, width = residual.shape
+    half = width // 2
+    chosen = expert_ids.shape[1]
+    low = mine * (expert_gate.shape[2] // 2)
+
+    pieces = [
+        packed(expert_gate[0], expert_up[0], expert_down[0], low + at)
+        for at in range(0, expert_gate.shape[2] // 2, PIECE)
+    ]
+    gathered = [lax.all_gather(piece, "sp", axis=0, tiled=True) for piece in pieces]
+
+    last_gated = (
+        linear_part[length - HALO :].astype(jnp.float32)
+        * jax.nn.sigmoid(gate_part[length - HALO :].astype(jnp.float32))
+    ).astype(jnp.bfloat16)
+    halo, halo_docs = passed_along((last_gated, documents[length - reach :]), "sp", 1)
+    docs = jnp.concatenate([halo_docs, documents], 0)
+    runs = sum(
+        (docs[reach - offset : reach - offset + length] == documents).astype(jnp.int32)
+        for offset in range(1, reach + 1)
+    )
+    short = (jnp.min(runs.reshape(length // 64, 64), 1) < reach).astype(jnp.int32)
+    taps = kernel_taps.astype(jnp.float32)
+
+    def conv_of(part):
+        own_runs = lax.dynamic_slice_in_dim(runs, part * rows, rows)
+        own_short = lax.dynamic_slice_in_dim(short, part * (rows // 64), rows // 64)
+        return convolve(
+            part[None],
+            linear_part,
+            gate_part,
+            halo,
+            taps,
+            jnp.broadcast_to(own_runs[:, None], (rows, LANES)),
+            own_short,
+        )
+
+    odd = lax.axis_index("sp") % 2
+    quarter = half // 2
+    fetched = swapped(lax.dynamic_slice_in_dim(output_weight, odd * quarter, quarter, 0), "tp")
+    theirs = conv_of(other)
+    came = swapped(theirs, "tp")
+    own = conv_of(mine)
+    fetched, own = lax.optimization_barrier((fetched, own))
+    beside = swapped(fetched, "sp")
+    w_came = jnp.concatenate([jnp.where(odd == 0, fetched, beside), jnp.where(odd == 0, beside, fetched)], 0)
+
+    gain = channel_gain[None, :]
+    own_gain = lax.dynamic_slice_in_dim(gain, mine * half, half, 1)
+    came_gain = lax.dynamic_slice_in_dim(gain, other * half, half, 1)
+    named = jnp.concatenate([expert_ids.T.astype(jnp.float32), route_weights.T], 0)
+    named_there = swapped(named, "tp")
+    table = weight_table(named[:chosen], named[chosen:])
+    table_there = weight_table(named_there[:chosen], named_there[chosen:])
+
+    part = rows // 2
+    gains = mix_gain[None, :]
+    normed, there = None, []
+    for at in (0, part):
+        normed = project(
+            at, part, own, came, own_gain, came_gain, output_weight, w_came, residual, gains, normed
+        )
+        there.append(swapped(lax.slice_in_dim(normed, at, at + part), "tp"))
+
+    common = (
+        jax.nn.silu(jnp.dot(normed, shared_gate, preferred_element_type=jnp.float32))
+        * jnp.dot(normed, shared_up, preferred_element_type=jnp.float32)
+    ).astype(jnp.bfloat16)
+    shared_out = jnp.dot(common, shared_down, preferred_element_type=jnp.float32)
+
+    here_sum = experts((0, rows), normed, table, gathered[0], None, jnp.float32)
+    there_sums = [
+        experts((0, part), there[k], table_there[k * part : (k + 1) * part], gathered[0], None, jnp.float32, (here_sum,))
+        for k in range(2)
+    ]
+    waited = (here_sum, *there_sums)
+    returned = []
+    for first, count in ((0, part // 2), (part // 2, part // 2), (part, part)):
+        k, at = divmod(first, part)
+        done = experts(
+            (at, count),
+            there[k],
+            table_there[k * part : (k + 1) * part],
+            gathered[1],
+            there_sums[k],
+            jnp.bfloat16,
+            waited,
+        )
+        returned.append(swapped(done, "tp"))
+    routed = experts((0, rows), normed, table, gathered[1], here_sum, jnp.float32, waited)
+    out, at = None, 0
+    for block in returned:
+        out = finish(at, normed, routed, shared_out, block, final_gain[None, :], out)
+        at += block.shape[0]
+    return out
+
+
+def shards(*arguments):
+    linear_part, kernel_taps, residual, expert_gate = [arguments[at] for at in (0, 2, 5, 10)]
+    splits = (
+        lax.axis_size("tp") == 2
+        and lax.axis_size("sp") % 4 == 0
+        and expert_gate.shape[0] == 1
+        and expert_gate.shape[2] == 4 * PIECE
+        and residual.shape[0] % 1024 == 0
+        and residual.shape[1] % 1024 == 0
+        and kernel_taps.shape[0] <= HALO
+    )
+    return shards_split(*arguments) if splits else shards_any(*arguments)
+
+
 def solution(mesh):
     return jax.shard_map(
         shards,

time: 755 us -> 403 us (0.53)
  waiting for transfers between devices: 351 us -> 86.9 us
  Pallas kernels: 0 us -> 240 us
  matrix products: 211 us -> 13.9 us
  other arithmetic: 126 us -> 11.7 us
  local copies, waits for them, and re-layouts: 33.7 us -> 21.6 us
    all_gather x5 -> x2, waiting for transfers between devices: 302 us -> 0.02 us  [shards_split(): lax.all_gather(piece, 'sp', axis=0, tiled=True)]
    pallas_call x0 -> x14, Pallas kernels: none -> 240 us  [the longest x7 166 us: experts(): pl.pallas_call(functools.partial(experts_kernel, group, piece, start is n...]
    dot_general x37 -> x2, matrix products: 211 us -> 13.9 us  [the longest x1 10.4 us: shards_split(): jnp.dot(common, shared_down, preferred_element_type=jnp.float32)]
    convert_element_type x6 -> x4, other arithmetic: 121 us -> 1.59 us  [the longest x1 0.92 us: shards_split(): last_gated = (linear_part[length - HALO:].astype(jnp.float32) * jax.nn.si...]
    ppermute x0 -> x9, waiting for transfers between devices: none -> 86.8 us  [swapped(): lax.ppermute(block, axis, [(i, i ^ 1) for i in range(lax.axis_size(axis))])]
    all_to_all x1 -> x0, waiting for transfers between devices: 46.5 us -> none  [shards(): lax.all_to_all(convolved, 'tp', split_axis=0, concat_axis=1, tiled=True)]
    unnamed x67 -> x28, local copies, waits for them, and re-layouts: 21.9 us -> 5.61 us
    ppermute x0 -> x9, starting transfers between devices: none -> 9.77 us  [swapped(): lax.ppermute(block, axis, [(i, i ^ 1) for i in range(lax.axis_size(axis))])]
  transfers between devices with their start and end apart: 8 -> 13, of which waited for: 5 -> 4; matrix products, arithmetic and copies ran while one was open for 45% -> 9% of each run, Pallas kernels for 0% -> 54%
where the time goes in v1:
time: 403 us
  Pallas kernels  240 us (60%)
  waiting for transfers between devices  86.9 us (22%)
  local copies, waits for them, and re-layouts  21.6 us (5%)
  starting transfers between devices  15.2 us (4%)
  matrix products  13.9 us (3%)
  between operations  13.7 us (3%)
  other arithmetic  11.7 us (3%)
    pallas_call x7, Pallas kernels, experts(): pl.pallas_call(functools.partial(experts_kernel, group, piece, start is n...  166 us
    ppermute x9, waiting for transfers between devices, swapped(): lax.ppermute(block, axis, [(i, i ^ 1) for i in range(lax.axis_size(axis))])  86.8 us
    pallas_call x2, Pallas kernels, convolve(): pl.pallas_call(functools.partial(conv_kernel, taps.shape[0]), out_shape=j...  34.1 us
    pallas_call x2, Pallas kernels, project(): pl.pallas_call(project_kernel, out_shape=jax.ShapeDtypeStruct((total_rows...  23.8 us
    pallas_call x3, Pallas kernels, finish(): pl.pallas_call(finish_kernel, out_shape=jax.ShapeDtypeStruct((rows, width...  15.5 us
    dot_general x1, matrix products, shards_split(): jnp.dot(common, shared_down, preferred_element_type=jnp.float32)  10.4 us
    ppermute x9, starting transfers between devices, swapped(): lax.ppermute(block, axis, [(i, i ^ 1) for i in range(lax.axis_size(axis))])  9.77 us
  transfers between devices with their start and end apart: 13, of which 4 were waited for; matrix products, arithmetic and copies ran while one was open for 9% of the time, Pallas kernels for 54%

profile of v1, /device:TPU:0, one launch (start us, length us, event | category | flops | bytes accessed | tf_op | source)
XLA Modules:
  0.0 402.6 jit_solution(5399086551834723554)
XLA Ops:
  6.5 1.4 constant_dynamic-slice_fusion
  7.9 0.3 copy.32
  8.2 0.2 copy.30
  8.4 1.7 dynamic-slice_bitcast_fusion
  10.1 1.3 pad_maximum_fusion.2
  11.4 0.0 all-gather.7.cloned.1.call-update
  11.5 0.0 all-gather.5.cloned.1.call-start
  11.5 0.3 copy.31
  11.8 0.2 copy.28
  12.0 1.3 pad_maximum_fusion.1
  13.3 0.0 all-gather.5.cloned.1.call-update
  13.4 1.7 constant_dynamic-slice_fusion.2
  15.1 3.1 collective-permute-start
  18.2 0.1 slice.146
  18.3 1.4 collective-permute-start.2
  19.7 0.9 multiply_convert_fusion.2
  20.6 4.0 collective-permute-start.1
  24.6 0.7 convert_element_type.117.tap_ref
  25.3 0.2 convert_add_fusion
  25.5 0.1 reshape.35
  25.5 0.1 reduce_min.9
  25.7 0.6 fusion.68
  26.3 1.0 broadcast_in_dim.74.runs_ref
  27.3 17.1 %convolve.2.own_ref = bf16[1024,1024]{1,0:T(8,128)(2,1)} custom-call(s32[1]{0:T(128)} %bitcast.part_ref, bf16[2048,1024]{1,0:T(8,128)(2,1)} %lin_back_ref.3, bf16[2048,1024]{1,0:T(8,128)(2,1)} %gate_back_ref.3, bf16[2048,1024]{1,0:T(8,128)(2,1)} %lin_back_ref.3, bf16[2048,1024]{1,0:T(8,128)(2,1)} %gate_back_ref.3, bf16[32,1024]{1,0:T(8,128)(2,1)} %copy-done.7, ...), custom_call_target="tpu_custom_call" | custom-call | flops 390070272 | bytes 6291456 | tf_op jit(solution)/shard_map/convolve/pallas_call | solution.py:239
  44.4 19.5 %collective-permute-done = bf16[512,2048]{1,0:T(8,128)(2,1)} collective-permute-done((bf16[512,2048]{1,0:T(8,128)(2,1)S(1)}, bf16[512,2048]{1,0:T(8,128)(2,1)}, u32[]{:S(2)}, u32[]{:S(2)}) %collective-permute-start) | collective-permute-done | bytes 2097184 | tf_op jit(solution)/shard_map/ppermute | solution.py:460
  64.0 1.8 collective-permute-start.6
  65.8 1.0 broadcast_in_dim.76.runs_ref
  66.8 17.1 %convolve.3 = bf16[1024,1024]{1,0:T(8,128)(2,1)} custom-call(s32[1]{0:T(128)} %bitcast.1.part_ref, bf16[2048,1024]{1,0:T(8,128)(2,1)} %lin_back_ref.3, bf16[2048,1024]{1,0:T(8,128)(2,1)} %gate_back_ref.3, bf16[2048,1024]{1,0:T(8,128)(2,1)} %lin_back_ref.3, bf16[2048,1024]{1,0:T(8,128)(2,1)} %gate_back_ref.3, bf16[32,1024]{1,0:T(8,128)(2,1)} %copy-done.7, ...), custom_call_target="tpu_custom_call" | custom-call | flops 390070272 | bytes 6291456 | tf_op jit(solution)/shard_map/convolve/pallas_call | solution.py:239
  83.8 0.4 collective-permute-start.3
  84.2 1.4 select_add_fusion.1.table_ref
  85.6 0.6 fusion.66
  86.3 0.6 select_add_fusion
  86.9 0.8 fusion.62
  87.7 2.6 broadcast_select_fusion.1
  90.3 2.6 pad_maximum_fusion.w_came_ref
  92.9 38.9 %collective-permute-done.3.came_ref = bf16[1024,1024]{1,0:T(8,128)(2,1)S(1)} collective-permute-done((bf16[1024,1024]{1,0:T(8,128)(2,1)}, bf16[1024,1024]{1,0:T(8,128)(2,1)S(1)}, u32[]{:S(2)}, u32[]{:S(2)}) %collective-permute-start.3) | collective-permute-done | bytes 2097184 | tf_op jit(solution)/shard_map/ppermute | solution.py:460
  131.8 1.3 copy-done.4
  133.1 11.6 %project.2.refs_0_ = bf16[1024,2048]{1,0:T(8,128)(2,1)} custom-call(bf16[1024,1024]{1,0:T(8,128)(2,1)} %convolve.2.own_ref, bf16[1024,1024]{1,0:T(8,128)(2,1)} %copy-done.4, f32[1,1024]{1,0:T(1,128)} %bitcast.53, f32[1,1024]{1,0:T(1,128)} %bitcast.51, bf16[1024,2048]{1,0:T(8,128)(2,1)} %w_own_ref.3, bf16[1024,2048]{1,0:T(8,128)(2,1)} %pad_maximum_fusion.w_came_ref, ...), custom_call_target="tpu_custom_call" | custom-call | flops 4294967296 | bytes 14680064 | tf_op jit(solution)/shard_map/project/pallas_call | solution.py:313
  144.7 3.2 slice.251
  148.0 0.3 collective-permute-start.5
  148.3 12.2 %project.3.x_ref.normed_ref = bf16[1024,2048]{1,0:T(8,128)(2,1)} custom-call(bf16[1024,1024]{1,0:T(8,128)(2,1)} %convolve.2.own_ref, bf16[1024,1024]{1,0:T(8,128)(2,1)} %copy-done.4, f32[1,1024]{1,0:T(1,128)} %bitcast.54, f32[1,1024]{1,0:T(1,128)} %bitcast.52, bf16[1024,2048]{1,0:T(8,128)(2,1)} %w_own_ref.3, ...), custom_call_target="tpu_custom_call", output_to_operand_aliasing={{}: (8, {})} | custom-call | flops 4294967296 | bytes 14680064 | tf_op jit(solution)/shard_map/project/pallas_call | solution.py:313
  160.4 3.3 slice.257
  163.8 1.6 collective-permute-start.7
  165.3 3.5 fusion.71
  168.8 10.4 %fusion.shared_ref = f32[1024,2048]{1,0:T(8,128)} fusion(bf16[256,2048]{1,0:T(8,128)(2,1)S(1)} %copy-done, f32[1024,256]{1,0:T(8,128)} %fusion.71, bf16[1024,2048]{1,0:T(8,128)(2,1)} %project.3.x_ref.normed_ref, bf16[2048,256]{1,0:T(8,128)(2,1)} %param.31), kind=kOutput, calls=%fused_computation.6 | convolution fusion | flops 2149056512 | bytes 15728640 | tf_op jit(solution)/shard_map/dot_general | solution.py:561
  179.2 35.5 %experts.7.refs_0_.refs_1_ = f32[1024,2048]{1,0:T(8,128)} custom-call(bf16[1024,2048]{1,0:T(8,128)(2,1)} %project.3.x_ref.normed_ref, f32[1024,128]{1,0:T(8,128)} %select_add_fusion.1.table_ref, bf16[16,3072,256]{2,1,0:T(8,128)(2,1)} %bitcast.67), custom_call_target="tpu_custom_call" | custom-call | flops 25769803776 | bytes 41943040 | tf_op jit(solution)/shard_map/experts/pallas_call | solution.py:393
  214.8 25.4 %collective-permute-done.7.x_ref = bf16[512,2048]{1,0:T(8,128)(2,1)} collective-permute-done((bf16[512,2048]{1,0:T(8,128)(2,1)}, bf16[512,2048]{1,0:T(8,128)(2,1)}, u32[]{:S(2)}, u32[]{:S(2)}) %collective-permute-start.7) | collective-permute-done | bytes 2097184 | tf_op jit(solution)/shard_map/ppermute | solution.py:460
  240.2 19.5 %experts.9.refs_3_.refs_0_ = f32[512,2048]{1,0:T(8,128)} custom-call(bf16[512,2048]{1,0:T(8,128)(2,1)} %collective-permute-done.7.x_ref, f32[512,128]{1,0:T(8,128)} %get-tuple-element.17.table_ref, bf16[16,3072,256]{2,1,0:T(8,128)(2,1)} %bitcast.68, f32[1024,2048]{1,0:T(8,128)} %experts.7.refs_0_.refs_1_), custom_call_target="tpu_custom_call" | custom-call | flops 12884901888 | bytes 33554432 | tf_op jit(solution)/shard_map/experts/pallas_call | solution.py:393
  259.7 1.4 copy-done.3
  261.0 19.5 %experts.8.refs_2_.refs_0_ = f32[512,2048]{1,0:T(8,128)} custom-call(bf16[512,2048]{1,0:T(8,128)(2,1)} %copy-done.3, f32[512,128]{1,0:T(8,128)} %get-tuple-element.18.table_ref, bf16[16,3072,256]{2,1,0:T(8,128)(2,1)} %bitcast.69, f32[1024,2048]{1,0:T(8,128)} %experts.7.refs_0_.refs_1_), custom_call_target="tpu_custom_call" | custom-call | flops 12884901888 | bytes 33554432 | tf_op jit(solution)/shard_map/experts/pallas_call | solution.py:393
  280.5 0.0 all-gather.5.cloned.1.call-done
  280.5 15.3 %experts.13 = bf16[256,2048]{1,0:T(8,128)(2,1)} custom-call(bf16[512,2048]{1,0:T(8,128)(2,1)} %copy-done.3, f32[512,128]{1,0:T(8,128)} %get-tuple-element.18.table_ref, bf16[16,3072,256]{2,1,0:T(8,128)(2,1)} %bitcast.40, f32[512,2048]{1,0:T(8,128)} %experts.8.refs_2_.refs_0_, f32[1024,2048]{1,0:T(8,128)} %experts.7.refs_0_.refs_1_, ...), custom_call_target="tpu_custom_call" | custom-call | flops 6442450944 | bytes 29360128 | tf_op jit(solution)/shard_map/experts/pallas_call | solution.py:393
  295.8 0.5 collective-permute-start.10
  296.3 15.3 %experts.12 = bf16[256,2048]{1,0:T(8,128)(2,1)} custom-call(bf16[512,2048]{1,0:T(8,128)(2,1)} %copy-done.3, f32[512,128]{1,0:T(8,128)} %get-tuple-element.18.table_ref, bf16[16,3072,256]{2,1,0:T(8,128)(2,1)} %bitcast.41, f32[512,2048]{1,0:T(8,128)} %experts.8.refs_2_.refs_0_, f32[1024,2048]{1,0:T(8,128)} %experts.7.refs_0_.refs_1_, ...), custom_call_target="tpu_custom_call" | custom-call | flops 6442450944 | bytes 29360128 | tf_op jit(solution)/shard_map/experts/pallas_call | solution.py:393
  311.6 1.7 collective-permute-start.9
  313.3 21.9 %experts.11 = bf16[512,2048]{1,0:T(8,128)(2,1)} custom-call(bf16[512,2048]{1,0:T(8,128)(2,1)} %collective-permute-done.7.x_ref, f32[512,128]{1,0:T(8,128)} %get-tuple-element.17.table_ref, bf16[16,3072,256]{2,1,0:T(8,128)(2,1)} %bitcast.42, f32[512,2048]{1,0:T(8,128)} %experts.9.refs_3_.refs_0_, f32[1024,2048]{1,0:T(8,128)} %experts.7.refs_0_.refs_1_, ...), custom_call_target="tpu_custom_call" | custom-call | flops 12884901888 | bytes 33554432 | tf_op jit(solution)/shard_map/experts/pallas_call | solution.py:393
  335.2 0.5 collective-permute-start.8
  335.7 39.2 %experts.10.routed_ref = f32[1024,2048]{1,0:T(8,128)} custom-call(bf16[1024,2048]{1,0:T(8,128)(2,1)} %project.3.x_ref.normed_ref, f32[1024,128]{1,0:T(8,128)} %select_add_fusion.1.table_ref, bf16[16,3072,256]{2,1,0:T(8,128)(2,1)} %bitcast.43, f32[1024,2048]{1,0:T(8,128)} %experts.7.refs_0_.refs_1_, f32[1024,2048]{1,0:T(8,128)} %experts.7.refs_0_.refs_1_, ...), custom_call_target="tpu_custom_call" | custom-call | flops 25769803776 | bytes 41943040 | tf_op jit(solution)/shard_map/experts/pallas_call | solution.py:393
  375.0 1.0 copy-done.6
  375.9 4.1 %finish.3.refs_0_ = bf16[1024,2048]{1,0:T(8,128)(2,1)} custom-call(bf16[1024,2048]{1,0:T(8,128)(2,1)} %project.3.x_ref.normed_ref, f32[1024,2048]{1,0:T(8,128)} %experts.10.routed_ref, f32[1024,2048]{1,0:T(8,128)} %fusion.shared_ref, bf16[256,2048]{1,0:T(8,128)(2,1)} %copy-done.6, f32[1,2048]{1,0:T(1,128)} %bitcast.48), custom_call_target="tpu_custom_call" | custom-call | flops 5242880 | bytes 7340032 | tf_op jit(solution)/shard_map/finish/pallas_call | solution.py:433
  380.1 4.1 %finish.4.refs_0_ = bf16[1024,2048]{1,0:T(8,128)(2,1)} custom-call(bf16[1024,2048]{1,0:T(8,128)(2,1)} %project.3.x_ref.normed_ref, f32[1024,2048]{1,0:T(8,128)} %experts.10.routed_ref, f32[1024,2048]{1,0:T(8,128)} %fusion.shared_ref, bf16[256,2048]{1,0:T(8,128)(2,1)} %collective-permute-done.9.came_ref, ...), custom_call_target="tpu_custom_call", output_to_operand_aliasing={{}: (5, {})} | custom-call | flops 5242880 | bytes 7340032 | tf_op jit(solution)/shard_map/finish/pallas_call | solution.py:433
  384.2 3.0 collective-permute-done.8.came_ref
  387.2 1.4 copy-done.5
  388.6 7.2 %finish.5 = bf16[1024,2048]{1,0:T(8,128)(2,1)} custom-call(bf16[1024,2048]{1,0:T(8,128)(2,1)} %project.3.x_ref.normed_ref, f32[1024,2048]{1,0:T(8,128)} %experts.10.routed_ref, f32[1024,2048]{1,0:T(8,128)} %fusion.shared_ref, bf16[512,2048]{1,0:T(8,128)(2,1)} %copy-done.5, f32[1,2048]{1,0:T(1,128)} %bitcast.50, ...), custom_call_target="tpu_custom_call", output_to_operand_aliasing={{}: (5, {})} | custom-call | flops 10485760 | bytes 14680064 | tf_op jit(solution)/shard_map/finish/pallas_call | solution.py:433
  (39 shorter events, 0.1 us)
Async XLA Ops:
  6.5 162.3 %copy-start = (bf16[256,2048]{1,0:T(8,128)(2,1)S(1)}, bf16[256,2048]{1,0:T(8,128)(2,1)}, u32[]{:S(2)}) copy-start(bf16[256,2048]{1,0:T(8,128)(2,1)} %param.32) | copy-start | bytes 3145732
  6.5 172.7 %all-gather.7.cloned.1.call-start = ((), (), s32[]{:S(2)}) async-start(), calls=%async_computation.1 | async-start | bytes 26738688 | tf_op jit(solution)/shard_map/all_gather | solution.py:502
  11.5 269.1 %all-gather.5.cloned.1.call-start = ((), (), s32[]{:S(2)}) async-start(), calls=%async_computation | async-start | bytes 26738688 | tf_op jit(solution)/shard_map/all_gather | solution.py:502
  13.3 4.8 %copy-start.10 = (s32[2048]{0:T(1024)S(1)}, s32[2048]{0:T(1024)}, u32[]{:S(2)}) copy-start(s32[2048]{0:T(1024)} %param.24) | copy-start | bytes 24580
  13.3 11.3 %copy-start.8 = (bf16[31,1024]{1,0:T(8,128)(2,1)S(1)}, bf16[31,1024]{1,0:T(8,128)(2,1)}, u32[]{:S(2)}) copy-start(bf16[31,1024]{1,0:T(8,128)(2,1)} %param.19) | copy-start | bytes 190468
  15.1 48.8 %collective-permute-start = (bf16[512,2048]{1,0:T(8,128)(2,1)S(1)}, bf16[512,2048]{1,0:T(8,128)(2,1)}, u32[]{:S(2)}, u32[]{:S(2)}) collective-permute-start(bf16[512,2048]{1,0:T(8,128)(2,1)S(1)} %constant_dynamic-slice_fusion.2), channel_id=1, source_target_pairs={{0,1},{1,0},{2,3},{3,2},{4,5},{5,4},{6,7},{7,6},{8,9},{9,8},{10,11... | collective-permute-start | bytes 6291464 | tf_op jit(solution)/shard_map/ppermute | solution.py:460
  18.3 7.0 %collective-permute-start.2 = (s32[30]{0:T(128)S(1)}, s32[30]{0:T(128)S(1)}, u32[]{:S(2)}, u32[]{:S(2)}) collective-permute-start(s32[30]{0:T(128)S(1)} %slice.146), channel_id=1, source_target_pairs={{0,2},{2,4},{4,6},{6,8},{8,10},{10,12},{12,14},{14,16},{16,18},{18... | collective-permute-start | bytes 368 | tf_op jit(solution)/shard_map/ppermute | solution.py:17
  20.6 5.7 %collective-permute-start.1 = (bf16[32,1024]{1,0:T(8,128)(2,1)S(1)}, bf16[32,1024]{1,0:T(8,128)(2,1)S(1)}, u32[]{:S(2)}, u32[]{:S(2)}) collective-permute-start(bf16[32,1024]{1,0:T(8,128)(2,1)S(1)} %multiply_convert_fusion.2), channel_id=1, source_target_pairs={{0,2},{2,4},{4,6},{6,8},{8,10},{10,12},{12,14},{14,16},{16,18},{18... | collective-permute-start | bytes 196616 | tf_op jit(solution)/shard_map/ppermute | solution.py:17
  26.3 1.0 copy-start.7
  27.3 36.6 %copy-start.11 = (s32[1024,2]{0,1:T(2,128)S(1)}, s32[1024,2]{0,1:T(2,128)}, u32[]{:S(2)}) copy-start(s32[1024,2]{0,1:T(2,128)} %param.25) | copy-start | bytes 24580
  27.3 36.6 %copy-start.9 = (f32[1024,2]{0,1:T(2,128)S(1)}, f32[1024,2]{0,1:T(2,128)}, u32[]{:S(2)}) copy-start(f32[1024,2]{0,1:T(2,128)} %param.26) | copy-start | bytes 24580
  63.9 23.8 %collective-permute-start.4 = (bf16[512,2048]{1,0:T(8,128)(2,1)}, bf16[512,2048]{1,0:T(8,128)(2,1)}, u32[]{:S(2)}, u32[]{:S(2)}) collective-permute-start(bf16[512,2048]{1,0:T(8,128)(2,1)} %collective-permute-done), channel_id=1, source_target_pairs={{0,2},{2,0},{4,6},{6,4},{8,10},{10,8},{12,14},{14,12},{16,18},{18,... | collective-permute-start | bytes 6291464 | tf_op jit(solution)/shard_map/ppermute | solution.py:460
  64.0 22.3 %collective-permute-start.6 = (f32[4,1024]{1,0:T(4,128)S(1)}, f32[4,1024]{1,0:T(4,128)S(1)}, u32[]{:S(2)}, u32[]{:S(2)}) collective-permute-start(f32[4,1024]{1,0:T(4,128)S(1)} %pad_maximum_fusion.3), channel_id=1, source_target_pairs={{0,1},{1,0},{2,3},{3,2},{4,5},{5,4},{6,7},{7,6},{8,9},{9,8},{10,11... | collective-permute-start | bytes 49160 | tf_op jit(solution)/shard_map/ppermute | solution.py:460
  66.8 18.9 %copy-start.12 = (f32[2048]{0:T(1024)S(1)}, f32[2048]{0:T(1024)}, u32[]{:S(2)}) copy-start(f32[2048]{0:T(1024)} %param.20) | copy-start | bytes 24580
  83.8 47.9 %collective-permute-start.3 = (bf16[1024,1024]{1,0:T(8,128)(2,1)}, bf16[1024,1024]{1,0:T(8,128)(2,1)S(1)}, u32[]{:S(2)}, u32[]{:S(2)}) collective-permute-start(bf16[1024,1024]{1,0:T(8,128)(2,1)} %convolve.3), channel_id=1, source_target_pairs={{0,1},{1,0},{2,3},{3,2},{4,5},{5,4},{6,7},{7,6},{8,9},{9,8},{10,11... | collective-permute-start | bytes 6291464 | tf_op jit(solution)/shard_map/ppermute | solution.py:460
  131.8 1.3 copy-start.4
  148.0 111.7 %collective-permute-start.5 = (bf16[512,2048]{1,0:T(8,128)(2,1)}, bf16[512,2048]{1,0:T(8,128)(2,1)S(1)}, u32[]{:S(2)}, u32[]{:S(2)}) collective-permute-start(bf16[512,2048]{1,0:T(8,128)(2,1)} %slice.251), channel_id=1, source_target_pairs={{0,1},{1,0},{2,3},{3,2},{4,5},{5,4},{6,7},{7,6},{8,9},{9,8},{10,11... | collective-permute-start | bytes 6291464 | tf_op jit(solution)/shard_map/ppermute | solution.py:460
  160.4 4.9 %copy-start.2 = (bf16[1024,2048]{1,0:T(8,128)(2,1)S(1)}, bf16[1024,2048]{1,0:T(8,128)(2,1)}, u32[]{:S(2)}) copy-start(bf16[1024,2048]{1,0:T(8,128)(2,1)} %project.3.x_ref.normed_ref) | copy-start | bytes 12582916
  163.8 76.4 %collective-permute-start.7 = (bf16[512,2048]{1,0:T(8,128)(2,1)}, bf16[512,2048]{1,0:T(8,128)(2,1)}, u32[]{:S(2)}, u32[]{:S(2)}) collective-permute-start(bf16[512,2048]{1,0:T(8,128)(2,1)} %slice.257), channel_id=1, source_target_pairs={{0,1},{1,0},{2,3},{3,2},{4,5},{5,4},{6,7},{7,6},{8,9},{9,8},{10,11... | collective-permute-start | bytes 6291464 | tf_op jit(solution)/shard_map/ppermute | solution.py:460
  259.6 1.4 copy-start.3
  295.8 79.1 %collective-permute-start.10 = (bf16[256,2048]{1,0:T(8,128)(2,1)}, bf16[256,2048]{1,0:T(8,128)(2,1)S(1)}, u32[]{:S(2)}, u32[]{:S(2)}) collective-permute-start(bf16[256,2048]{1,0:T(8,128)(2,1)} %experts.13), channel_id=1, source_target_pairs={{0,1},{1,0},{2,3},{3,2},{4,5},{5,4},{6,7},{7,6},{8,9},{9,8},{10,11... | collective-permute-start | bytes 3145736 | tf_op jit(solution)/shard_map/ppermute | solution.py:460
  311.6 68.5 %collective-permute-start.9 = (bf16[256,2048]{1,0:T(8,128)(2,1)}, bf16[256,2048]{1,0:T(8,128)(2,1)}, u32[]{:S(2)}, u32[]{:S(2)}) collective-permute-start(bf16[256,2048]{1,0:T(8,128)(2,1)} %experts.12), channel_id=1, source_target_pairs={{0,1},{1,0},{2,3},{3,2},{4,5},{5,4},{6,7},{7,6},{8,9},{9,8},{10,11... | collective-permute-start | bytes 3145736 | tf_op jit(solution)/shard_map/ppermute | solution.py:460
  335.2 52.0 %collective-permute-start.8 = (bf16[512,2048]{1,0:T(8,128)(2,1)}, bf16[512,2048]{1,0:T(8,128)(2,1)S(1)}, u32[]{:S(2)}, u32[]{:S(2)}) collective-permute-start(bf16[512,2048]{1,0:T(8,128)(2,1)} %experts.11), channel_id=1, source_target_pairs={{0,1},{1,0},{2,3},{3,2},{4,5},{5,4},{6,7},{7,6},{8,9},{9,8},{10,11... | collective-permute-start | bytes 6291464 | tf_op jit(solution)/shard_map/ppermute | solution.py:460
  375.0 1.0 copy-start.6
  387.2 1.4 copy-start.5
  388.6 7.2 %copy-start.1 = (bf16[256,2048]{1,0:T(8,128)(2,1)S(1)}, bf16[256,2048]{1,0:T(8,128)(2,1)}, u32[]{:S(2)}) copy-start(bf16[256,2048]{1,0:T(8,128)(2,1)} %param.32) | copy-start | bytes 3145732
Sparse Core Ops, SparseCore 0:
  11.6 131.2 all-gather.6
  144.5 129.2 all-gather.4
